TPU v7x, 512 devices: a whole 4x8x8 slice. The times are simulated.
512 devices in a mesh: sp: 32 (over z, x), tp: 16 (over y, core).
Axes of the slice: x: 4, y: 8, z: 8, core: 2. Of those that a mesh axis runs over, the one named last changes fastest.
Arguments:
- cotangent: bfloat16 [4096, 2048], P('sp'), may hold values from -6 to 6
- mixer_out: bfloat16 [4096, 2048], P('sp'), may hold values from -6 to 6
- expert_ids: int32 [4096, 2], P('sp'), may hold values from 0 to 31, all different within a row; in each aligned block of 128 rows (0 to 127, 128 to 255, ...) at most 16 rows name the same one
- route_weight: float32 [4096, 2], P('sp'), may hold values from 0.3 to 1.5
- saved_normalized: bfloat16 [4096, 2048], P('sp', 'tp'), may hold values from -6 to 6
- inverse_deviation: float32 [4096], P('sp'), may hold values from 0.3 to 3
- channel_norm_gain: float32 [2048], P('tp'), may hold values from 0.1 to 1.9
- taps: float32 [31, 2048], P(None, 'tp'), may hold values from -1 to 1
- proj_weight: bfloat16 [2048, 2048], P('tp'), may hold values from -0.125 to 0.125
- gate_weight: bfloat16 [32, 2048, 2048], P('sp', None, 'tp'), may hold values from -0.125 to 0.125
- up_weight: bfloat16 [32, 2048, 2048], P('sp', None, 'tp'), may hold values from -0.125 to 0.125
- down_weight: bfloat16 [32, 2048, 2048], P('sp', 'tp'), may hold values from -0.125 to 0.125
Outputs:
- grad_mixer_in: bfloat16 [4096, 2048], P('sp', 'tp')
- grad_proj: float32 [2048, 2048], P('sp', 'tp')
- grad_gate: bfloat16 [32, 2048, 2048], P('sp', None, 'tp')
- grad_up: bfloat16 [32, 2048, 2048], P('sp', None, 'tp')
- grad_down: bfloat16 [32, 2048, 2048], P('sp', 'tp')
Inputs may be any that keep to these rules, and one draw needn't show every extreme that they name: `expert_ids`: each row names 2 different experts. Within the rows of one index of sp no expert is named more than 16 times, a bound that some block reaches.
All inputs are finite; a program needn't handle non-finite values.
Results may differ from a plain program's by a relative error of at most 0.02.
Values may be sent and summed in bfloat16 or wider, within the bound.
No kernel may reach another device: no remote copies, remote signals or barrier semaphores. Data moves between devices by JAX's collectives and lax.ppermute only.
A program may use at most 64 MiB of HBM per device.

v0:
```python
import jax
import jax.numpy as jnp
from jax import lax
from jax.sharding import PartitionSpec as P


def sent_together(arrays, axis, split_dim, concat_dim, along):
    both = jnp.concatenate(arrays, axis=along)
    filled, at, finished = (
        lax.all_to_all(both, axis, split_axis=split_dim, concat_axis=concat_dim, tiled=True),
        0,
        [],
    )
    for a in arrays:
        finished.append(lax.slice_in_dim(filled, at, at + a.shape[along], axis=along))
        at += a.shape[along]
    return tuple(finished)


def side_by_side(arrays, axis, dim, along):
    ends, at = ([], 0)
    for a in arrays[:-1]:
        at += a.shape[along]
        ends.append(at)
    both = jnp.concatenate(arrays, axis=along)
    return tuple(jnp.split(lax.all_gather(both, axis, axis=dim, tiled=True), ends, axis=along))


def in_blocks(value, dim, size):
    dims = value.shape
    pieces = value.reshape(*dims[:dim], size, dims[dim] // size, *dims[dim + 1 :])
    return jnp.moveaxis(pieces, dim, 0)


def sent_and_summed(value, axis, dim):
    pieces = in_blocks(value, dim, lax.axis_size(axis))
    arrived = lax.all_to_all(pieces, axis, split_axis=0, concat_axis=0, tiled=True)
    return arrived.astype(jnp.float32).sum(axis=0)


def sent_to_all(value, axis):
    size = lax.axis_size(axis)
    return lax.all_to_all(
        jnp.broadcast_to(value[None], (size, *value.shape)), axis, 0, 0, tiled=True
    )


def taken_together(value, axis):
    everything = sent_to_all(value, axis)
    return jnp.sum(everything, axis=0)


def packed_total(arrays, axis):
    ends = [0]
    for a in arrays:
        ends.append(ends[-1] + a.size)
    running = taken_together(jnp.concatenate([a.ravel() for a in arrays]), axis)
    return tuple((running[b:e].reshape(a.shape) for a, b, e in zip(arrays, ends, ends[1:])))


def from_behind(value, axis, steps):
    count = lax.axis_size(axis)
    leading, last = (max(0, -steps), min(count, count - steps))
    return lax.ppermute(value, axis, [(source, source + steps) for source in range(leading, last)])


def route_table(expert_ids, route_weight, slot_start, slot_span, capacity, experts):
    onehot = (expert_ids[:, :, None] == jnp.arange(experts, dtype=jnp.int32)[None, None, :]).astype(
        jnp.int32
    )
    flat_hot = onehot.reshape(-1, experts)
    ranks = jnp.cumsum(flat_hot, axis=0) - flat_hot
    rank_pair = jnp.sum(ranks * flat_hot, axis=1).reshape(expert_ids.shape)
    slot_index = expert_ids * capacity + rank_pair
    targets = (
        jnp.arange(experts, dtype=jnp.int32)[:, None] * capacity
        + slot_start
        + jnp.arange(slot_span, dtype=jnp.int32)[None, :]
    ).reshape(-1)
    matched = slot_index[None, :, :] == targets[:, None, None]
    dispatch = jnp.any(matched, axis=2).astype(jnp.bfloat16)
    slot_weight = jnp.sum(jnp.where(matched, route_weight[None, :, :], 0.0), axis=(1, 2))
    return (dispatch, slot_weight)


def shards(
    cotangent,
    mixer_out,
    expert_ids,
    route_weight,
    saved_normalized,
    inverse_deviation,
    channel_norm_gain,
    taps,
    proj_weight,
    gate_weight,
    up_weight,
    down_weight,
):
    experts = lax.axis_size("sp")
    groups = lax.axis_size("tp")
    tok_rows, model_width = cotangent.shape
    capacity = groups * max(1, 4 * tok_rows // (experts * groups))
    slot_span = capacity // groups
    slot_start = lax.axis_index("tp") * slot_span
    dispatch, slot_weight = route_table(
        expert_ids, route_weight, slot_start, slot_span, capacity, experts
    )
    sent_rows = jnp.dot(dispatch, mixer_out, preferred_element_type=jnp.float32).astype(
        jnp.bfloat16
    )
    sent_grad = (
        slot_weight[:, None] * jnp.dot(dispatch, cotangent, preferred_element_type=jnp.float32)
    ).astype(jnp.bfloat16)
    sent_rows = sent_rows.reshape(experts, slot_span, model_width)
    sent_grad = sent_grad.reshape(experts, slot_span, model_width)
    shared_rows = sent_together((sent_rows, sent_grad), "sp", 0, 0, 1)
    routed_rows, routed_grad = side_by_side((shared_rows[0], shared_rows[1]), "tp", 1, 0)
    full_table, unused_weight = route_table(
        expert_ids, route_weight, 0, capacity, capacity, experts
    )
    routed_rows = routed_rows.reshape(-1, model_width)
    routed_grad = routed_grad.reshape(-1, model_width)
    w_first = gate_weight[0]
    w_third = up_weight[0]
    w_second = down_weight[0]
    contract_last = (((1,), (1,)), ((), ()))
    contract_first = (((0,), (0,)), ((), ()))
    hidden_gate = jnp.dot(routed_rows, w_first, preferred_element_type=jnp.float32)
    hidden_up = jnp.dot(routed_rows, w_third, preferred_element_type=jnp.float32)
    sigma = jax.nn.sigmoid(hidden_gate)
    swish = hidden_gate * sigma
    activ = (swish * hidden_up).astype(jnp.bfloat16)
    grad_second = lax.dot_general(
        activ, routed_grad, contract_first, preferred_element_type=jnp.float32
    ).astype(jnp.bfloat16)
    grad_activ = lax.dot_general(
        routed_grad, w_second, contract_last, preferred_element_type=jnp.float32
    )
    grad_gpre = (grad_activ * hidden_up * sigma * (1.0 + hidden_gate * (1.0 - sigma))).astype(
        jnp.bfloat16
    )
    grad_upre = (grad_activ * swish).astype(jnp.bfloat16)
    grad_first = lax.dot_general(
        routed_rows, grad_gpre, contract_first, preferred_element_type=jnp.float32
    ).astype(jnp.bfloat16)
    grad_third = lax.dot_general(
        routed_rows, grad_upre, contract_first, preferred_element_type=jnp.float32
    ).astype(jnp.bfloat16)
    partial_value = lax.dot_general(
        grad_gpre, w_first, contract_last, preferred_element_type=jnp.float32
    ) + lax.dot_general(grad_upre, w_third, contract_last, preferred_element_type=jnp.float32)
    scattered = sent_and_summed(partial_value.astype(jnp.bfloat16), "tp", 1).astype(jnp.bfloat16)
    home_parts = lax.all_to_all(
        scattered.reshape(experts, capacity, -1), "sp", split_axis=0, concat_axis=0, tiled=True
    )
    home_rows = lax.all_gather(home_parts, "tp", axis=2, tiled=True)
    returned = lax.dot_general(
        full_table,
        home_rows.reshape(-1, model_width),
        contract_first,
        preferred_element_type=jnp.float32,
    )
    mixer_grad = (cotangent.astype(jnp.float32) + returned).astype(jnp.bfloat16)
    normalized_input = saved_normalized.astype(jnp.float32)
    normalized_values = normalized_input * channel_norm_gain[None, :]
    gate_sig = jax.nn.sigmoid(normalized_values)
    act_conv = (normalized_values * gate_sig).astype(jnp.bfloat16)
    grad_proj = sent_and_summed(
        lax.dot_general(
            mixer_grad, act_conv, contract_first, preferred_element_type=jnp.float32
        ).astype(jnp.bfloat16),
        "sp",
        0,
    )
    grad_act = lax.dot_general(
        mixer_grad, proj_weight, contract_last, preferred_element_type=jnp.float32
    )
    norm_output_gradient = (
        grad_act
        * gate_sig
        * (1.0 + normalized_values * (1.0 - gate_sig))
        * channel_norm_gain[None, :]
    )
    reduced_totals = packed_total(
        (
            jnp.sum(norm_output_gradient, axis=1),
            jnp.sum(norm_output_gradient * normalized_input, axis=1),
        ),
        "tp",
    )
    channel_count = saved_normalized.shape[1] * groups
    conv_output_gradient = inverse_deviation[:, None] * (
        norm_output_gradient
        - reduced_totals[0][:, None] / channel_count
        - normalized_input * (reduced_totals[1][:, None] / channel_count)
    )
    reach = taps.shape[0] - 1
    beyond = from_behind(conv_output_gradient[:reach], "sp", -1)
    extended = jnp.concatenate([conv_output_gradient, beyond], axis=0)
    result = jnp.zeros_like(conv_output_gradient)
    for tap_index in range(taps.shape[0]):
        result = result + taps[tap_index][None, :] * extended[tap_index : tap_index + tok_rows]
    return (
        result.astype(jnp.bfloat16),
        grad_proj,
        grad_first[None],
        grad_third[None],
        grad_second[None],
    )


def solution(mesh):
    return jax.shard_map(
        shards,
        mesh=mesh,
        in_specs=(
            P("sp", None),
            P("sp", None),
            P("sp", None),
            P("sp", None),
            P("sp", "tp"),
            P("sp"),
            P("tp"),
            P(None, "tp"),
            P("tp", None),
            P("sp", None, "tp"),
            P("sp", None, "tp"),
            P("sp", "tp", None),
        ),
        out_specs=(
            P("sp", "tp"),
            P("sp", "tp"),
            P("sp", None, "tp"),
            P("sp", None, "tp"),
            P("sp", "tp", None),
        ),
        check_vma=False,
    )
```

profile of v0, /device:TPU:1, one launch (start us, length us, event | category | flops | bytes accessed | tf_op | source)
XLA Modules:
  0.0 256.7 jit_solution(6382690411300353336)
XLA Ops:
  7.2 0.8 copy.64
  8.4 0.6 reduce-window.6
  9.5 0.7 multiply_add_fusion
  10.3 0.5 copy-done.9
  10.8 0.9 fusion.123
  11.6 1.2 fusion.5
  12.9 1.2 fusion.6
  14.2 0.3 copy.68
  14.5 24.8 %all_to_all.26 = bf16[32,2,2048]{2,1,0:T(2,128)(2,1)S(1)} all-to-all(bf16[32,2,2048]{2,1,0:T(2,128)(2,1)S(1)} %copy.68), channel_id=1, replica_groups=mesh['sp'=32,'tp'=16] {'sp'}, dimensions={0} | all-to-all | bytes 524288 | tf_op jit(solution)/shard_map/all_to_all | solution.py:10
  39.3 0.4 fusion.134
  39.6 0.7 pad_maximum_fusion
  40.3 0.9 copy.69
  41.3 42.1 %all-gather.3.cloned.1.call-done = bf16[64,16,2048]{2,0,1:T(8,128)(2,1)} async-done(((bf16[64,1,2048]{2,0,1:T(8,128)(2,1)}), bf16[64,16,2048]{2,0,1:T(8,128)(2,1)}) %all-gather.3.cloned.1.call-update) | async-done | bytes 4194320 | tf_op jit(solution)/shard_map/all_gather | solution.py:26
  83.4 2.7 %fusion.133 = (bf16[32,16,2048]{2,0,1:T(8,128)(2,1)S(1)}, bf16[32,16,2048]{2,0,1:T(8,128)(2,1)S(1)}) fusion(bf16[64,16,2048]{2,0,1:T(8,128)(2,1)} %all-gather.3.cloned.1.call-done), kind=kLoop, calls=%fused_computation.256 | loop fusion | bytes 8388608 | tf_op jit(solution)/shard_map/split | solution.py:26
  86.1 1.2 copy.75
  87.3 1.2 copy.76
  88.5 0.7 fusion.12
  89.2 0.3 copy-done.4
  89.5 0.7 fusion.15
  90.2 0.3 copy-done.39
  90.5 0.7 multiply_convert_fusion.1
  91.3 0.7 fusion.10
  92.0 0.7 fusion.7
  92.7 0.5 copy.83
  93.3 55.3 %all_to_all.27 = bf16[16,512,128]{2,1,0:T(8,128)(2,1)} all-to-all(bf16[16,512,128]{2,1,0:T(8,128)(2,1)S(1)} %bitcast.144), channel_id=1, replica_groups=mesh['sp'=32,'tp'=16] {'tp'}, dimensions={0} | all-to-all | bytes 4194304 | tf_op jit(solution)/shard_map/all_to_all | solution.py:37
  148.5 2.6 reduce_sum.72
  151.1 20.5 %all_to_all.28 = bf16[32,16,128]{2,1,0:T(8,128)(2,1)} all-to-all(bf16[32,16,128]{2,1,0:T(8,128)(2,1)} %bitcast.146), channel_id=1, replica_groups=mesh['sp'=32,'tp'=16] {'sp'}, dimensions={0} | all-to-all | bytes 262144 | tf_op jit(solution)/shard_map/all_to_all | solution.py:154
  171.7 0.7 add.148
  172.4 1.5 compare_reduce_fusion
  173.9 1.6 slice_bitcast_fusion.29
  175.4 1.6 slice_bitcast_fusion.30
  177.1 3.0 %fusion.3 = bf16[1,128,2048]{2,1,0:T(8,128)(2,1)} fusion(bf16[512,2048]{1,0:T(8,128)(2,1)} %bitcast.143, f32[512,128]{1,0:T(8,128)} %copy-done.5, f32[512,128]{1,0:T(8,128)S(1)} %fusion.12), kind=kOutput, calls=%fused_computation.9 | convolution fusion | flops 269090816 | bytes 3145728 | tf_op jit(solution)/shard_map/dot_general | solution.py:134
  180.1 26.1 %all-gather.5.cloned.1.call-done = bf16[32,16,2048]{2,1,0:T(8,128)(2,1)} async-done(((bf16[32,16,128]{2,1,0:T(8,128)(2,1)}), bf16[32,16,2048]{2,1,0:T(8,128)(2,1)}) %all-gather.5.cloned.1.call-update) | async-done | bytes 2097168 | tf_op jit(solution)/shard_map/all_gather | solution.py:157
  206.2 2.2 fusion
  208.4 0.8 copy-done.3
  209.2 0.4 fusion.132
  209.6 0.6 broadcast_in_dim.22
  210.2 5.1 %all-to-all-start.3 = ((f32[16,1,256]{2,1,0:T(1,128)}), f32[16,1,256]{2,1,0:T(1,128)S(1)}, u32[]{:S(2)}, u32[]{:S(2)}) async-start(f32[16,1,256]{2,1,0:T(1,128)} %broadcast_in_dim.22), calls=%async_computation.3 | async-start | bytes 32768 | tf_op jit(solution)/shard_map/all_to_all | solution.py:43
  215.3 2.2 convolution_convert_fusion.3
  217.5 5.2 %all-to-all-done.3 = f32[16,1,256]{2,1,0:T(1,128)S(1)} async-done(((f32[16,1,256]{2,1,0:T(1,128)}), f32[16,1,256]{2,1,0:T(1,128)S(1)}, u32[]{:S(2)}, u32[]{:S(2)}) %all-to-all-start.3) | async-done | bytes 16416 | tf_op jit(solution)/shard_map/all_to_all | solution.py:43
  222.7 9.9 %all-to-all-start.4 = ((bf16[32,64,128]{2,1,0:T(8,128)(2,1)}), bf16[32,64,128]{2,1,0:T(8,128)(2,1)S(1)}, u32[]{:S(2)}, u32[]{:S(2)}) async-start(bf16[32,64,128]{2,1,0:T(8,128)(2,1)} %bitcast.42), calls=%async_computation.4 | async-start | bytes 1048576 | tf_op jit(solution)/shard_map/all_to_all | solution.py:37
  232.6 1.6 fusion.2
  234.6 1.3 collective-permute-start
  235.9 1.6 fusion.1
  237.5 2.3 collective-permute-done
  240.0 0.8 fusion.35
  240.9 8.3 %all-to-all-done.4 = bf16[32,64,128]{2,1,0:T(8,128)(2,1)S(1)} async-done(((bf16[32,64,128]{2,1,0:T(8,128)(2,1)}), bf16[32,64,128]{2,1,0:T(8,128)(2,1)S(1)}, u32[]{:S(2)}, u32[]{:S(2)}) %all-to-all-start.4) | async-done | bytes 524320 | tf_op jit(solution)/shard_map/all_to_all | solution.py:37
  249.2 0.7 convert_reduce_fusion
  (101 shorter events, 1.5 us)
Async XLA Ops:
  7.2 81.3 %copy-start = (bf16[1,2048,128]{2,1,0:T(8,128)(2,1)S(1)}, bf16[1,2048,128]{2,1,0:T(8,128)(2,1)}, u32[]{:S(2)}) copy-start(bf16[1,2048,128]{2,1,0:T(8,128)(2,1)} %param.21) | copy-start | bytes 1572868
  7.2 76.2 %all-gather.3.cloned.1.call-start = ((), (), s32[]{:S(2)}) async-start(), calls=%async_computation.5 | async-start | bytes 4456448 | tf_op jit(solution)/shard_map/all_gather | solution.py:26
  10.2 0.6 copy-start.9
  41.2 165.0 %all-gather.5.cloned.1.call-start = ((), (), s32[]{:S(2)}) async-start(), calls=%async_computation.6 | async-start | bytes 2228224 | tf_op jit(solution)/shard_map/all_gather | solution.py:157
  87.3 3.0 %copy-start.1 = (bf16[32,16,2048]{2,1,0:T(8,128)(2,1)}, bf16[32,16,2048]{2,1,0:T(8,128)(2,1)S(1)}, u32[]{:S(2)}) copy-start(bf16[32,16,2048]{2,1,0:T(8,128)(2,1)S(1)} %copy.75) | copy-start | bytes 6291460
  88.4 1.0 copy-start.4
  89.5 1.0 copy-start.39
  90.2 1.0 copy-start.5
  91.3 0.7 copy-start.6
  151.1 55.1 %copy-start.2 = (bf16[128,2048]{1,0:T(8,128)(2,1)S(1)}, bf16[128,2048]{1,0:T(8,128)(2,1)}, u32[]{:S(2)}) copy-start(bf16[128,2048]{1,0:T(8,128)(2,1)} %param.12) | copy-start | bytes 1572868
  180.1 29.1 %copy-start.8 = (bf16[128,128]{1,0:T(8,128)(2,1)S(1)}, bf16[128,128]{1,0:T(8,128)(2,1)}, u32[]{:S(2)}) copy-start(bf16[128,128]{1,0:T(8,128)(2,1)} %param.16) | copy-start | bytes 98308
  180.1 29.1 %copy-start.37 = (f32[128]{0:T(128)S(1)}, f32[128]{0:T(128)}, u32[]{:S(2)}) copy-start(f32[128]{0:T(128)} %param.18) | copy-start | bytes 1540
  206.2 3.0 %copy-start.40 = (bf16[128,2048]{1,0:T(8,128)(2,1)S(1)}, bf16[128,2048]{1,0:T(8,128)(2,1)}, u32[]{:S(2)}) copy-start(bf16[128,2048]{1,0:T(8,128)(2,1)} %param.20) | copy-start | bytes 1572868
  208.3 0.8 copy-start.3
  209.2 23.4 %copy-start.7 = (bf16[512,128]{1,0:T(8,128)(2,1)S(1)}, bf16[512,128]{1,0:T(8,128)(2,1)}, u32[]{:S(2)}) copy-start(bf16[512,128]{1,0:T(8,128)(2,1)} %copy-done.6) | copy-start | bytes 393220
  210.2 12.5 %all-to-all-start.3 = ((f32[16,1,256]{2,1,0:T(1,128)}), f32[16,1,256]{2,1,0:T(1,128)S(1)}, u32[]{:S(2)}, u32[]{:S(2)}) async-start(f32[16,1,256]{2,1,0:T(1,128)} %broadcast_in_dim.22), calls=%async_computation.3 | async-start | bytes 32768 | tf_op jit(solution)/shard_map/all_to_all | solution.py:43
  222.7 26.5 %all-to-all-start.4 = ((bf16[32,64,128]{2,1,0:T(8,128)(2,1)}), bf16[32,64,128]{2,1,0:T(8,128)(2,1)S(1)}, u32[]{:S(2)}, u32[]{:S(2)}) async-start(bf16[32,64,128]{2,1,0:T(8,128)(2,1)} %bitcast.42), calls=%async_computation.4 | async-start | bytes 1048576 | tf_op jit(solution)/shard_map/all_to_all | solution.py:37
  232.6 1.6 copy-start.38
  234.3 5.4 %copy-start.10 = (f32[128]{0:T(128)S(1)}, f32[128]{0:T(128)}, u32[]{:S(2)}) copy-start(f32[128]{0:T(128)} %get-tuple-element.36) | copy-start | bytes 1540
  234.3 5.4 %copy-start.11 = (f32[128]{0:T(128)S(1)}, f32[128]{0:T(128)}, u32[]{:S(2)}) copy-start(f32[128]{0:T(128)} %get-tuple-element.37) | copy-start | bytes 1540
  234.4 5.4 %copy-start.12 = (f32[128]{0:T(128)S(1)}, f32[128]{0:T(128)}, u32[]{:S(2)}) copy-start(f32[128]{0:T(128)} %get-tuple-element.38) | copy-start | bytes 1540
  234.4 5.4 %copy-start.13 = (f32[128]{0:T(128)S(1)}, f32[128]{0:T(128)}, u32[]{:S(2)}) copy-start(f32[128]{0:T(128)} %get-tuple-element.39) | copy-start | bytes 1540
  234.4 5.4 %copy-start.14 = (f32[128]{0:T(128)S(1)}, f32[128]{0:T(128)}, u32[]{:S(2)}) copy-start(f32[128]{0:T(128)} %get-tuple-element.40) | copy-start | bytes 1540
  234.4 5.4 %copy-start.15 = (f32[128]{0:T(128)S(1)}, f32[128]{0:T(128)}, u32[]{:S(2)}) copy-start(f32[128]{0:T(128)} %get-tuple-element.41) | copy-start | bytes 1540
  234.4 5.4 %copy-start.16 = (f32[128]{0:T(128)S(1)}, f32[128]{0:T(128)}, u32[]{:S(2)}) copy-start(f32[128]{0:T(128)} %get-tuple-element.42) | copy-start | bytes 1540
  234.4 5.4 %copy-start.17 = (f32[128]{0:T(128)S(1)}, f32[128]{0:T(128)}, u32[]{:S(2)}) copy-start(f32[128]{0:T(128)} %get-tuple-element.43) | copy-start | bytes 1540
  234.4 5.4 %copy-start.18 = (f32[128]{0:T(128)S(1)}, f32[128]{0:T(128)}, u32[]{:S(2)}) copy-start(f32[128]{0:T(128)} %get-tuple-element.13) | copy-start | bytes 1540
  234.4 5.4 %copy-start.19 = (f32[128]{0:T(128)S(1)}, f32[128]{0:T(128)}, u32[]{:S(2)}) copy-start(f32[128]{0:T(128)} %get-tuple-element.14) | copy-start | bytes 1540
  234.4 5.4 %copy-start.20 = (f32[128]{0:T(128)S(1)}, f32[128]{0:T(128)}, u32[]{:S(2)}) copy-start(f32[128]{0:T(128)} %get-tuple-element.15) | copy-start | bytes 1540
  234.4 5.4 %copy-start.21 = (f32[128]{0:T(128)S(1)}, f32[128]{0:T(128)}, u32[]{:S(2)}) copy-start(f32[128]{0:T(128)} %get-tuple-element.16) | copy-start | bytes 1540
  234.5 5.4 %copy-start.22 = (f32[128]{0:T(128)S(1)}, f32[128]{0:T(128)}, u32[]{:S(2)}) copy-start(f32[128]{0:T(128)} %get-tuple-element.17) | copy-start | bytes 1540
  234.5 5.4 %copy-start.23 = (f32[128]{0:T(128)S(1)}, f32[128]{0:T(128)}, u32[]{:S(2)}) copy-start(f32[128]{0:T(128)} %get-tuple-element.18) | copy-start | bytes 1540
  234.5 5.4 %copy-start.24 = (f32[128]{0:T(128)S(1)}, f32[128]{0:T(128)}, u32[]{:S(2)}) copy-start(f32[128]{0:T(128)} %get-tuple-element.19) | copy-start | bytes 1540
  234.5 5.4 %copy-start.25 = (f32[128]{0:T(128)S(1)}, f32[128]{0:T(128)}, u32[]{:S(2)}) copy-start(f32[128]{0:T(128)} %get-tuple-element.20) | copy-start | bytes 1540
  234.5 5.4 %copy-start.26 = (f32[128]{0:T(128)S(1)}, f32[128]{0:T(128)}, u32[]{:S(2)}) copy-start(f32[128]{0:T(128)} %get-tuple-element.21) | copy-start | bytes 1540
  234.5 5.4 %copy-start.27 = (f32[128]{0:T(128)S(1)}, f32[128]{0:T(128)}, u32[]{:S(2)}) copy-start(f32[128]{0:T(128)} %get-tuple-element.22) | copy-start | bytes 1540
  234.5 5.4 %copy-start.28 = (f32[128]{0:T(128)S(1)}, f32[128]{0:T(128)}, u32[]{:S(2)}) copy-start(f32[128]{0:T(128)} %get-tuple-element.23) | copy-start | bytes 1540
  234.5 5.4 %copy-start.29 = (f32[128]{0:T(128)S(1)}, f32[128]{0:T(128)}, u32[]{:S(2)}) copy-start(f32[128]{0:T(128)} %get-tuple-element.24) | copy-start | bytes 1540
  234.5 5.4 %copy-start.30 = (f32[128]{0:T(128)S(1)}, f32[128]{0:T(128)}, u32[]{:S(2)}) copy-start(f32[128]{0:T(128)} %get-tuple-element.25) | copy-start | bytes 1540
  234.5 5.4 %copy-start.31 = (f32[128]{0:T(128)S(1)}, f32[128]{0:T(128)}, u32[]{:S(2)}) copy-start(f32[128]{0:T(128)} %get-tuple-element.26) | copy-start | bytes 1540
  234.6 5.4 %copy-start.32 = (f32[128]{0:T(128)S(1)}, f32[128]{0:T(128)}, u32[]{:S(2)}) copy-start(f32[128]{0:T(128)} %get-tuple-element.27) | copy-start | bytes 1540
  234.6 5.4 %copy-start.33 = (f32[128]{0:T(128)S(1)}, f32[128]{0:T(128)}, u32[]{:S(2)}) copy-start(f32[128]{0:T(128)} %get-tuple-element.28) | copy-start | bytes 1540
  234.6 5.4 %copy-start.34 = (f32[128]{0:T(128)S(1)}, f32[128]{0:T(128)}, u32[]{:S(2)}) copy-start(f32[128]{0:T(128)} %get-tuple-element.29) | copy-start | bytes 1540
  234.6 5.4 %copy-start.35 = (f32[128]{0:T(128)S(1)}, f32[128]{0:T(128)}, u32[]{:S(2)}) copy-start(f32[128]{0:T(128)} %get-tuple-element.30) | copy-start | bytes 1540
  234.6 5.4 %copy-start.36 = (f32[128]{0:T(128)S(1)}, f32[128]{0:T(128)}, u32[]{:S(2)}) copy-start(f32[128]{0:T(128)} %get-tuple-element.31) | copy-start | bytes 1540
  234.6 5.2 %collective-permute-start = (f32[30,128]{1,0:T(8,128)S(1)}, f32[30,128]{1,0:T(8,128)S(1)}, u32[]{:S(2)}, u32[]{:S(2)}) collective-permute-start(f32[30,128]{1,0:T(8,128)S(1)} %slice.275), channel_id=1, source_target_pairs={{16,0},{32,16},{48,32},{64,48},{80,64},{96,80},{112,96},{128,112},... | collective-permute-start | bytes 46088 | tf_op jit(solution)/shard_map/ppermute | solution.py:64
Sparse Core Ops, SparseCore 0:
  41.3 42.0 all-gather.2
  171.8 34.3 all-gather.4
where the time goes:
time: 258 us; the launch traced here: 257 us
  blocking collectives  101 us (39%)
  waiting for transfers between devices  84 us (33%)
  matrix products  16.9 us (7%)
  starting transfers between devices  16.4 us (6%)
  local copies, waits for them, and re-layouts  15.1 us (6%)
  between operations  14.8 us (6%)
  other arithmetic  8.92 us (3%)
    all_to_all x1, blocking collectives, sent_and_summed(): lax.all_to_all(pieces, axis, split_axis=0, concat_axis=0, tiled=True)  55.3 us
    all_gather x1, waiting for transfers between devices, side_by_side(): lax.all_gather(both, axis, axis=dim, tiled=True)  42.1 us
    all_gather x1, waiting for transfers between devices, shards(): home_rows = lax.all_gather(home_parts, 'tp', axis=2, tiled=True)  26.1 us
    all_to_all x1, blocking collectives, sent_together(): lax.all_to_all(both, axis, split_axis=split_dim, concat_axis=concat_dim,...  24.8 us
    all_to_all x1, blocking collectives, shards(): lax.all_to_all(scattered.reshape(experts, capacity, -1), 'sp', split_axis...  20.5 us
    all_to_all x1, starting transfers between devices, sent_and_summed(): lax.all_to_all(pieces, axis, split_axis=0, concat_axis=0, tiled=True)  9.9 us
    all_to_all x1, waiting for transfers between devices, sent_and_summed(): lax.all_to_all(pieces, axis, split_axis=0, concat_axis=0, tiled=True)  8.31 us
    unnamed x85, local copies, waits for them, and re-layouts  5.2 us
  transfers between devices with their start and end apart: 5, of which 5 were waited for; matrix products, arithmetic and copies ran while one was open for 6% of the time, Pallas kernels for 0%

commit v1 on v0

--- a/solution.py
+++ b/solution.py
@@ -154,7 +154,8 @@
     home_parts = lax.all_to_all(
         scattered.reshape(experts, capacity, -1), "sp", split_axis=0, concat_axis=0, tiled=True
     )
-    home_rows = lax.all_gather(home_parts, "tp", axis=2, tiled=True)
+    sent = jnp.stack([home_parts] * lax.axis_size("tp"))
+    home_rows = jnp.concatenate(lax.all_to_all(sent, "tp", 0, 0), axis=2)
     returned = lax.dot_general(
         full_table,
         home_rows.reshape(-1, model_width),

time: 258 us -> 273 us (1.058)
  waiting for transfers between devices: 84 us -> 101 us
  local copies, waits for them, and re-layouts: 15.1 us -> 17.9 us
    all_to_all x0 -> x1, waiting for transfers between devices: none -> 43.5 us  [shards(): home_rows = jnp.concatenate(lax.all_to_all(sent, 'tp', 0, 0), axis=2)]
    all_gather x1 -> x0, waiting for transfers between devices: 26.1 us -> none  [shards(): home_rows = lax.all_gather(home_parts, 'tp', axis=2, tiled=True)]
    all_to_all x1, starting transfers between devices: 9.9 us -> 3.89 us  [sent_and_summed(): lax.all_to_all(pieces, axis, split_axis=0, concat_axis=0, tiled=True)]
    all_to_all x0 -> x1, starting transfers between devices: none -> 4.65 us  [shards(): home_rows = jnp.concatenate(lax.all_to_all(sent, 'tp', 0, 0), axis=2)]
    reshape x0 -> x1, local copies, waits for them, and re-layouts: none -> 4.08 us  [shards(): home_rows = jnp.concatenate(lax.all_to_all(sent, 'tp', 0, 0), axis=2)]
  transfers between devices with their start and end apart: 5 -> 5, of which waited for: 5 -> 5; matrix products, arithmetic and copies ran while one was open for 6% -> 4% of each run, Pallas kernels for 0% -> 0%
where the time goes in v1:
time: 273 us; the launch traced here: 272 us
  waiting for transfers between devices  101 us (37%)
  blocking collectives  100 us (37%)
  local copies, waits for them, and re-layouts  17.9 us (7%)
  starting transfers between devices  15.3 us (6%)
  matrix products  15.1 us (6%)
  between operations  14.7 us (5%)
  other arithmetic  7.55 us (3%)
    all_to_all x1, blocking collectives, sent_and_summed(): lax.all_to_all(pieces, axis, split_axis=0, concat_axis=0, tiled=True)  55.3 us
    all_to_all x1, waiting for transfers between devices, shards(): home_rows = jnp.concatenate(lax.all_to_all(sent, 'tp', 0, 0), axis=2)  43.5 us
    all_gather x1, waiting for transfers between devices, side_by_side(): lax.all_gather(both, axis, axis=dim, tiled=True)  42.2 us
    all_to_all x1, blocking collectives, sent_together(): lax.all_to_all(both, axis, split_axis=split_dim, concat_axis=concat_dim,...  24.8 us
    all_to_all x1, blocking collectives, shards(): lax.all_to_all(scattered.reshape(experts, capacity, -1), 'sp', split_axis...  20.1 us
    all_to_all x1, waiting for transfers between devices, sent_and_summed(): lax.all_to_all(pieces, axis, split_axis=0, concat_axis=0, tiled=True)  7.87 us
  transfers between devices with their start and end apart: 5, of which 5 were waited for; matrix products, arithmetic and copies ran while one was open for 4% of the time, Pallas kernels for 0%

profile of v1, /device:TPU:1, one launch (start us, length us, event | category | flops | bytes accessed | tf_op | source)
XLA Modules:
  0.0 271.7 jit_solution(6538250690136339697)
XLA Ops:
  7.2 0.8 copy.67
  8.4 0.6 reduce-window.6
  9.5 0.7 multiply_add_fusion
  10.3 0.9 fusion.125
  11.2 1.2 fusion.5
  12.4 1.2 fusion.6
  14.0 24.8 %all_to_all.31 = bf16[32,2,2048]{2,1,0:T(2,128)(2,1)S(1)} all-to-all(bf16[32,2,2048]{2,1,0:T(2,128)(2,1)S(1)} %copy.71), channel_id=1, replica_groups=mesh['sp'=32,'tp'=16] {'sp'}, dimensions={0} | all-to-all | bytes 524288 | tf_op jit(solution)/shard_map/all_to_all | solution.py:10
  38.8 0.4 fusion.136
  39.2 0.7 pad_maximum_fusion
  39.8 0.9 copy.72
  40.7 42.2 %all-gather.2.cloned.1.call-done = bf16[64,16,2048]{2,0,1:T(8,128)(2,1)} async-done(((bf16[64,1,2048]{2,0,1:T(8,128)(2,1)}), bf16[64,16,2048]{2,0,1:T(8,128)(2,1)}) %all-gather.2.cloned.1.call-update) | async-done | bytes 4194320 | tf_op jit(solution)/shard_map/all_gather | solution.py:26
  82.9 2.7 %fusion.135 = (bf16[32,16,2048]{2,0,1:T(8,128)(2,1)S(1)}, bf16[32,16,2048]{2,0,1:T(8,128)(2,1)S(1)}) fusion(bf16[64,16,2048]{2,0,1:T(8,128)(2,1)} %all-gather.2.cloned.1.call-done), kind=kLoop, calls=%fused_computation.258 | loop fusion | bytes 8388608 | tf_op jit(solution)/shard_map/split | solution.py:26
  85.6 1.2 copy.79
  86.8 1.2 copy.80
  88.0 0.7 fusion.14
  88.7 0.3 copy-done.2
  89.0 0.7 fusion.17
  89.7 0.3 copy-done.31
  90.0 0.7 multiply_convert_fusion.1
  90.8 0.7 fusion.12
  91.5 0.7 fusion.9
  92.2 0.5 copy.92
  92.8 55.3 %all_to_all.32 = bf16[16,512,128]{2,1,0:T(8,128)(2,1)} all-to-all(bf16[16,512,128]{2,1,0:T(8,128)(2,1)S(1)} %bitcast.148), channel_id=1, replica_groups=mesh['sp'=32,'tp'=16] {'tp'}, dimensions={0} | all-to-all | bytes 4194304 | tf_op jit(solution)/shard_map/all_to_all | solution.py:37
  148.0 1.9 reduce_sum.72
  149.9 20.1 %all_to_all.33 = bf16[32,16,128]{2,1,0:T(8,128)(2,1)S(1)} all-to-all(bf16[32,16,128]{2,1,0:T(8,128)(2,1)S(1)} %bitcast.150), channel_id=1, replica_groups=mesh['sp'=32,'tp'=16] {'sp'}, dimensions={0} | all-to-all | bytes 262144 | tf_op jit(solution)/shard_map/all_to_all | solution.py:154
  170.0 1.7 stack.2
  171.7 4.7 %all-to-all-start.3 = ((bf16[16,32,16,128]{3,2,1,0:T(8,128)(2,1)}), bf16[16,32,16,128]{3,2,1,0:T(8,128)(2,1)}, u32[]{:S(2)}, u32[]{:S(2)}) async-start(bf16[16,32,16,128]{3,2,1,0:T(8,128)(2,1)} %stack.2), calls=%async_computation.3 | async-start | bytes 4194304 | tf_op jit(solution)/shard_map/all_to_all | solution.py:158
  176.7 0.6 slice_bitcast_fusion.29
  177.3 0.7 slice_bitcast_fusion.30
  178.0 2.9 %fusion.3 = bf16[1,128,2048]{2,1,0:T(8,128)(2,1)} fusion(bf16[512,2048]{1,0:T(8,128)(2,1)} %bitcast.147, f32[512,128]{1,0:T(8,128)S(1)} %fusion.17, f32[512,128]{1,0:T(8,128)S(1)} %fusion.14), kind=kOutput, calls=%fused_computation.9 | convolution fusion | flops 269090816 | bytes 3145728 | tf_op jit(solution)/shard_map/dot_general | solution.py:134
  180.9 43.5 %all-to-all-done.3 = bf16[16,32,16,128]{3,2,1,0:T(8,128)(2,1)} async-done(((bf16[16,32,16,128]{3,2,1,0:T(8,128)(2,1)}), bf16[16,32,16,128]{3,2,1,0:T(8,128)(2,1)}, u32[]{:S(2)}, u32[]{:S(2)}) %all-to-all-start.3) | async-done | bytes 2097184 | tf_op jit(solution)/shard_map/all_to_all | solution.py:158
  224.4 4.1 %copy.76 = bf16[32,16,16,128]{3,2,1,0:T(8,128)(2,1)S(1)} copy(bf16[32,16,16,128]{3,1,0,2:T(8,128)(2,1)} %bitcast.11) | data formatting | bytes 4194304 | tf_op jit(solution)/shard_map/reshape | solution.py:158
  228.5 0.5 fusion
  229.0 0.8 copy-done.4
  229.8 0.4 fusion.134
  230.2 0.6 broadcast_in_dim.22
  230.8 5.5 %all-to-all-start.4 = ((f32[16,1,256]{2,1,0:T(1,128)}), f32[16,1,256]{2,1,0:T(1,128)S(1)}, u32[]{:S(2)}, u32[]{:S(2)}) async-start(f32[16,1,256]{2,1,0:T(1,128)} %broadcast_in_dim.22), calls=%async_computation.4 | async-start | bytes 32768 | tf_op jit(solution)/shard_map/all_to_all | solution.py:43
  236.3 2.2 convolution_convert_fusion.3
  238.5 5.2 %all-to-all-done.4 = f32[16,1,256]{2,1,0:T(1,128)S(1)} async-done(((f32[16,1,256]{2,1,0:T(1,128)}), f32[16,1,256]{2,1,0:T(1,128)S(1)}, u32[]{:S(2)}, u32[]{:S(2)}) %all-to-all-start.4) | async-done | bytes 16416 | tf_op jit(solution)/shard_map/all_to_all | solution.py:43
  243.6 3.9 %all-to-all-start.5 = ((bf16[32,64,128]{2,1,0:T(8,128)(2,1)}), bf16[32,64,128]{2,1,0:T(8,128)(2,1)S(1)}, u32[]{:S(2)}, u32[]{:S(2)}) async-start(bf16[32,64,128]{2,1,0:T(8,128)(2,1)} %bitcast.42), calls=%async_computation.5 | async-start | bytes 1048576 | tf_op jit(solution)/shard_map/all_to_all | solution.py:37
  247.5 1.6 fusion.2
  249.1 0.8 fusion.32
  250.2 1.3 collective-permute-start
  251.5 1.6 fusion.1
  253.0 2.2 collective-permute-done
  255.5 0.8 fusion.37
  256.3 7.9 %all-to-all-done.5 = bf16[32,64,128]{2,1,0:T(8,128)(2,1)S(1)} async-done(((bf16[32,64,128]{2,1,0:T(8,128)(2,1)}), bf16[32,64,128]{2,1,0:T(8,128)(2,1)S(1)}, u32[]{:S(2)}, u32[]{:S(2)}) %all-to-all-start.5) | async-done | bytes 524320 | tf_op jit(solution)/shard_map/all_to_all | solution.py:37
  264.2 0.7 convert_reduce_fusion
  (86 shorter events, 1.7 us)
Async XLA Ops:
  7.2 80.8 %copy-start = (bf16[1,2048,128]{2,1,0:T(8,128)(2,1)S(1)}, bf16[1,2048,128]{2,1,0:T(8,128)(2,1)}, u32[]{:S(2)}) copy-start(bf16[1,2048,128]{2,1,0:T(8,128)(2,1)} %param.21) | copy-start | bytes 1572868
  7.2 75.7 %all-gather.2.cloned.1.call-start = ((), (), s32[]{:S(2)}) async-start(), calls=%async_computation.6 | async-start | bytes 4456448 | tf_op jit(solution)/shard_map/all_gather | solution.py:26
  86.8 2.9 %copy-start.1 = (bf16[32,16,2048]{2,1,0:T(8,128)(2,1)}, bf16[32,16,2048]{2,1,0:T(8,128)(2,1)S(1)}, u32[]{:S(2)}) copy-start(bf16[32,16,2048]{2,1,0:T(8,128)(2,1)S(1)} %copy.79) | copy-start | bytes 6291460
  88.0 1.0 copy-start.2
  89.0 1.0 copy-start.31
  171.7 5.0 %copy-start.6 = (f32[31,128]{1,0:T(8,128)S(1)}, f32[31,128]{1,0:T(8,128)}, u32[]{:S(2)}) copy-start(f32[31,128]{1,0:T(8,128)} %param.19) | copy-start | bytes 47620
  171.7 52.6 %all-to-all-start.3 = ((bf16[16,32,16,128]{3,2,1,0:T(8,128)(2,1)}), bf16[16,32,16,128]{3,2,1,0:T(8,128)(2,1)}, u32[]{:S(2)}, u32[]{:S(2)}) async-start(bf16[16,32,16,128]{3,2,1,0:T(8,128)(2,1)} %stack.2), calls=%async_computation.3 | async-start | bytes 4194304 | tf_op jit(solution)/shard_map/all_to_all | solution.py:158
  224.4 4.1 %copy-start.3 = (bf16[128,2048]{1,0:T(8,128)(2,1)S(1)}, bf16[128,2048]{1,0:T(8,128)(2,1)}, u32[]{:S(2)}) copy-start(bf16[128,2048]{1,0:T(8,128)(2,1)} %param.12) | copy-start | bytes 1572868
  228.5 1.4 copy-start.5
  228.5 1.3 copy-start.30
  228.5 1.3 copy-start.32
  229.0 0.8 copy-start.4
  230.8 12.8 %all-to-all-start.4 = ((f32[16,1,256]{2,1,0:T(1,128)}), f32[16,1,256]{2,1,0:T(1,128)S(1)}, u32[]{:S(2)}, u32[]{:S(2)}) async-start(f32[16,1,256]{2,1,0:T(1,128)} %broadcast_in_dim.22), calls=%async_computation.4 | async-start | bytes 32768 | tf_op jit(solution)/shard_map/all_to_all | solution.py:43
  243.6 20.6 %all-to-all-start.5 = ((bf16[32,64,128]{2,1,0:T(8,128)(2,1)}), bf16[32,64,128]{2,1,0:T(8,128)(2,1)S(1)}, u32[]{:S(2)}, u32[]{:S(2)}) async-start(bf16[32,64,128]{2,1,0:T(8,128)(2,1)} %bitcast.42), calls=%async_computation.5 | async-start | bytes 1048576 | tf_op jit(solution)/shard_map/all_to_all | solution.py:37
  249.9 5.3 %copy-start.7 = (f32[128]{0:T(128)S(1)}, f32[128]{0:T(128)}, u32[]{:S(2)}) copy-start(f32[128]{0:T(128)} %get-tuple-element.40) | copy-start | bytes 1540
  249.9 5.3 %copy-start.8 = (f32[128]{0:T(128)S(1)}, f32[128]{0:T(128)}, u32[]{:S(2)}) copy-start(f32[128]{0:T(128)} %get-tuple-element.41) | copy-start | bytes 1540
  250.0 5.3 %copy-start.9 = (f32[128]{0:T(128)S(1)}, f32[128]{0:T(128)}, u32[]{:S(2)}) copy-start(f32[128]{0:T(128)} %get-tuple-element.42) | copy-start | bytes 1540
  250.0 5.3 %copy-start.10 = (f32[128]{0:T(128)S(1)}, f32[128]{0:T(128)}, u32[]{:S(2)}) copy-start(f32[128]{0:T(128)} %get-tuple-element.43) | copy-start | bytes 1540
  250.0 5.3 %copy-start.11 = (f32[128]{0:T(128)S(1)}, f32[128]{0:T(128)}, u32[]{:S(2)}) copy-start(f32[128]{0:T(128)} %get-tuple-element.13) | copy-start | bytes 1540
  250.0 5.3 %copy-start.12 = (f32[128]{0:T(128)S(1)}, f32[128]{0:T(128)}, u32[]{:S(2)}) copy-start(f32[128]{0:T(128)} %get-tuple-element.14) | copy-start | bytes 1540
  250.0 5.3 %copy-start.13 = (f32[128]{0:T(128)S(1)}, f32[128]{0:T(128)}, u32[]{:S(2)}) copy-start(f32[128]{0:T(128)} %get-tuple-element.15) | copy-start | bytes 1540
  250.0 5.3 %copy-start.14 = (f32[128]{0:T(128)S(1)}, f32[128]{0:T(128)}, u32[]{:S(2)}) copy-start(f32[128]{0:T(128)} %get-tuple-element.16) | copy-start | bytes 1540
  250.0 5.3 %copy-start.15 = (f32[128]{0:T(128)S(1)}, f32[128]{0:T(128)}, u32[]{:S(2)}) copy-start(f32[128]{0:T(128)} %get-tuple-element.17) | copy-start | bytes 1540
  250.0 5.3 %copy-start.16 = (f32[128]{0:T(128)S(1)}, f32[128]{0:T(128)}, u32[]{:S(2)}) copy-start(f32[128]{0:T(128)} %get-tuple-element.18) | copy-start | bytes 1540
  250.0 5.3 %copy-start.17 = (f32[128]{0:T(128)S(1)}, f32[128]{0:T(128)}, u32[]{:S(2)}) copy-start(f32[128]{0:T(128)} %get-tuple-element.19) | copy-start | bytes 1540
  250.0 5.3 %copy-start.18 = (f32[128]{0:T(128)S(1)}, f32[128]{0:T(128)}, u32[]{:S(2)}) copy-start(f32[128]{0:T(128)} %get-tuple-element.20) | copy-start | bytes 1540
  250.1 5.3 %copy-start.19 = (f32[128]{0:T(128)S(1)}, f32[128]{0:T(128)}, u32[]{:S(2)}) copy-start(f32[128]{0:T(128)} %get-tuple-element.21) | copy-start | bytes 1540
  250.1 5.3 %copy-start.20 = (f32[128]{0:T(128)S(1)}, f32[128]{0:T(128)}, u32[]{:S(2)}) copy-start(f32[128]{0:T(128)} %get-tuple-element.22) | copy-start | bytes 1540
  250.1 5.3 %copy-start.21 = (f32[128]{0:T(128)S(1)}, f32[128]{0:T(128)}, u32[]{:S(2)}) copy-start(f32[128]{0:T(128)} %get-tuple-element.23) | copy-start | bytes 1540
  250.1 5.3 %copy-start.22 = (f32[128]{0:T(128)S(1)}, f32[128]{0:T(128)}, u32[]{:S(2)}) copy-start(f32[128]{0:T(128)} %get-tuple-element.24) | copy-start | bytes 1540
  250.1 5.3 %copy-start.23 = (f32[128]{0:T(128)S(1)}, f32[128]{0:T(128)}, u32[]{:S(2)}) copy-start(f32[128]{0:T(128)} %get-tuple-element.25) | copy-start | bytes 1540
  250.1 5.3 %copy-start.24 = (f32[128]{0:T(128)S(1)}, f32[128]{0:T(128)}, u32[]{:S(2)}) copy-start(f32[128]{0:T(128)} %get-tuple-element.26) | copy-start | bytes 1540
  250.1 5.3 %copy-start.25 = (f32[128]{0:T(128)S(1)}, f32[128]{0:T(128)}, u32[]{:S(2)}) copy-start(f32[128]{0:T(128)} %get-tuple-element.27) | copy-start | bytes 1540
  250.1 5.3 %copy-start.26 = (f32[128]{0:T(128)S(1)}, f32[128]{0:T(128)}, u32[]{:S(2)}) copy-start(f32[128]{0:T(128)} %get-tuple-element.28) | copy-start | bytes 1540
  250.1 5.3 %copy-start.27 = (f32[128]{0:T(128)S(1)}, f32[128]{0:T(128)}, u32[]{:S(2)}) copy-start(f32[128]{0:T(128)} %get-tuple-element.29) | copy-start | bytes 1540
  250.1 5.3 %copy-start.28 = (f32[128]{0:T(128)S(1)}, f32[128]{0:T(128)}, u32[]{:S(2)}) copy-start(f32[128]{0:T(128)} %get-tuple-element.30) | copy-start | bytes 1540
  250.2 5.3 %copy-start.29 = (f32[128]{0:T(128)S(1)}, f32[128]{0:T(128)}, u32[]{:S(2)}) copy-start(f32[128]{0:T(128)} %get-tuple-element.31) | copy-start | bytes 1540
  250.2 5.1 %collective-permute-start = (f32[30,128]{1,0:T(8,128)S(1)}, f32[30,128]{1,0:T(8,128)S(1)}, u32[]{:S(2)}, u32[]{:S(2)}) collective-permute-start(f32[30,128]{1,0:T(8,128)S(1)} %slice.275), channel_id=1, source_target_pairs={{16,0},{32,16},{48,32},{64,48},{80,64},{96,80},{112,96},{128,112},... | collective-permute-start | bytes 46088 | tf_op jit(solution)/shard_map/ppermute | solution.py:64
Sparse Core Ops, SparseCore 0:
  40.8 42.0 all-gather.1
